TPU v7x, 128 devices: a whole 4x4x4 slice. The times are simulated.
128 devices in a mesh: rep: 2 (over z_hi), fs: 32 (over z_lo, y, x), tp: 2 (over core).
Axes of the slice: x: 4, y: 4, z: 4 (z_hi: 2, z_lo: 2; z = z_hi * 2 + z_lo), core: 2. Of those that a mesh axis runs over, the one named last changes fastest.
Arguments:
- tokens: bfloat16 [256, 64, 2048], P('tp', ('rep', 'fs')), may hold values from -6 to 6
- mix_gain: float32 [2048], replicated, may hold values from 0.1 to 1.9
- value_weight: bfloat16 [2048, 1024], P('fs', 'tp'), may hold values from -0.125 to 0.125
- gate_weight: bfloat16 [2048, 1024], P('fs', 'tp'), may hold values from -0.125 to 0.125
- conv_taps: float32 [31, 1024], P(None, 'tp'), may hold values from -1 to 1
- head_gain: float32 [1024], P('tp'), may hold values from 0.1 to 1.9
- out_weight: bfloat16 [1024, 2048], P('tp', 'fs'), may hold values from -0.1875 to 0.1875
- ffn_gain: float32 [2048], replicated, may hold values from 0.1 to 1.9
- ffn_gate_weight: bfloat16 [2048, 3072], P('fs', 'tp'), may hold values from -0.125 to 0.125
- ffn_up_weight: bfloat16 [2048, 3072], P('fs', 'tp'), may hold values from -0.125 to 0.125
- down_weight: bfloat16 [3072, 2048], P('tp', 'fs'), may hold values from -0.109375 to 0.109375
Outputs:
- layer_out: bfloat16 [256, 64, 2048], P('tp', ('rep', 'fs'))
All inputs are finite; a program needn't handle non-finite values.
Results may differ from a plain program's by a relative error of at most 0.012.
Values may be sent and summed in bfloat16 or wider, within the bound.
No kernel may reach another device: no remote copies, remote signals or barrier semaphores. Data moves between devices by JAX's collectives and lax.ppermute only.
A program may use at most 128 MiB of HBM per device.

v0:
```python
import jax
import jax.numpy as jnp
from jax import lax
from jax.experimental import pallas as pl
from jax.experimental.pallas import tpu as pltpu
from jax.sharding import Mesh, PartitionSpec as P


HALO = 16
norm_eps = 1e-06
group_eps = 1e-05

Z = ("zh", "zl")
FS = ("zl", "y", "x")
SHIFTS = (1, 3, 2)
f32 = jnp.float32
bf16 = jnp.bfloat16
VMEM_LIMIT = 48 * 1024 * 1024


def swap(value, axis):
    return lax.ppermute(value, axis, [(0, 1), (1, 0)])


def shift_z(value, by):
    return lax.ppermute(value, Z, [(i, (i + by) % 4) for i in range(4)])


def ring(value, axis):
    got = [value]
    for d in SHIFTS:
        got.append(lax.ppermute(value, axis, [(i, (i + d) % 4) for i in range(4)]))
    return got


def two_ways(pair):
    along_x = jnp.stack(ring(pair[0], "x"))
    along_y = jnp.stack(ring(pair[1], "y"))
    return ring(along_x, "y"), ring(along_y, "x")


def ordered(first, second, widths):
    offs = (0, *SHIFTS)
    me = jnp.stack([lax.axis_index("y"), lax.axis_index("x")]).astype(jnp.int32)
    n = len(widths)

    def kernel(at, *refs):
        src, out, sem = refs[:8], refs[8 : 8 + n], refs[-1]
        copies = []
        for jy in range(4):
            y = lax.rem(at[0] + 4 - offs[jy], 4)
            for jx in range(4):
                x = lax.rem(at[1] + 4 - offs[jx], 4)
                for zl, ref in ((0, src[jy].at[jx]), (1, src[4 + jx].at[jy])):
                    start = 0
                    for k, w in enumerate(widths):
                        copies.append(
                            pltpu.make_async_copy(
                                ref.at[:, start : start + w], out[k].at[zl, y, x], sem.at[len(copies)]
                            )
                        )
                        copies[-1].start()
                        start += w
        for copy in copies:
            copy.wait()

    return pl.pallas_call(
        kernel,
        out_shape=[jax.ShapeDtypeStruct((2, 4, 4, 64, w), bf16) for w in widths],
        in_specs=[pl.BlockSpec(memory_space=pltpu.SMEM)] + [pl.BlockSpec(memory_space=pltpu.HBM)] * 8,
        out_specs=[pl.BlockSpec(memory_space=pltpu.VMEM)] * n,
        scratch_shapes=[pltpu.SemaphoreType.DMA((32 * n,))],
        cost_estimate=pl.CostEstimate(flops=1 << 30, transcendentals=0, bytes_accessed=1 << 22),
        compiler_params=pltpu.CompilerParams(vmem_limit_bytes=VMEM_LIMIT),
    )(me, *first, *second)


def mm(a, b):
    return jnp.dot(a, b, preferred_element_type=f32)


def mm_t(a, b):
    return lax.dot_general(a, b, (((1,), (1,)), ((), ())), preferred_element_type=f32)


def whole_call(kernel, outs, args, scratch=(), flops=0):
    specs = [
        pl.BlockSpec(memory_space=pltpu.SMEM) if a.dtype == jnp.int32 else pl.BlockSpec(memory_space=pltpu.VMEM)
        for a in args
    ]
    out_specs = [pl.BlockSpec(memory_space=pltpu.VMEM) for _ in outs]
    return pl.pallas_call(
        kernel,
        out_shape=[jax.ShapeDtypeStruct(s, d) for s, d in outs],
        in_specs=specs,
        out_specs=out_specs,
        scratch_shapes=list(scratch),
        cost_estimate=pl.CostEstimate(flops=flops, transcendentals=0, bytes_accessed=1 << 20),
        compiler_params=pltpu.CompilerParams(vmem_limit_bytes=VMEM_LIMIT),
    )(*args)


def k_blocks():
    return [(zl, y, zl * 1024 + y * 256) for zl in range(2) for y in range(4)]


def times_rows(x, w_ref):
    cols = w_ref.shape[-1]
    acc = jnp.zeros((x.shape[0], cols), f32)
    for zl, y, at in k_blocks():
        acc = acc + mm(x[:, at : at + 256], w_ref[zl, y].reshape(256, cols))
    return acc


def glu_kernel(x0, x1, x2, x3, gain, wa, wb, out):
    for i, x in enumerate((x0, x1, x2, x3)):
        rows = x[...].astype(f32)
        scale = lax.rsqrt(jnp.mean(rows * rows, axis=-1, keepdims=True) + norm_eps)
        normed = (rows * scale * gain[...]).astype(bf16)
        for j, w in enumerate((wa, wb)):
            both = times_rows(normed, w)
            half = both.shape[1] // 2
            out[i, :, j * half : (j + 1) * half] = (both[:, :half] * jax.nn.sigmoid(both[:, half:])).astype(bf16)


def conv_kernel(tp, glu, edge, small, out, pad):
    seqs, rows, chans = glu.shape
    half = chans // 2
    taps = small.shape[0] - 1
    left = jnp.where(tp[0] == 1, 1.0, 0.0).astype(f32)
    right = 1.0 - left
    chunk = 32

    def one(s, carry):
        near = edge[s].astype(f32)
        near = jnp.concatenate([near[:, half:], near[:, :half]], axis=1)
        pad[0:HALO] = near * left
        pad[HALO : HALO + rows] = glu[s].astype(f32)
        pad[HALO + rows :] = near * right
        for c in range(2):
            lanes = slice(c * half, (c + 1) * half)
            gain = small[taps : taps + 1, lanes]
            for r in range(0, rows, chunk):
                acc = jnp.zeros((chunk, half), f32)
                for k in range(taps):
                    at = r + k + HALO - taps // 2
                    acc = acc + small[k : k + 1, lanes] * pad[at : at + chunk, lanes]
                mean = jnp.mean(acc, axis=-1, keepdims=True)
                off = acc - mean
                var = jnp.mean(off * off, axis=-1, keepdims=True)
                scaled = off * lax.rsqrt(var + group_eps) * gain
                out[s, r : r + chunk, lanes] = (scaled * jax.nn.sigmoid(scaled)).astype(bf16)
        return carry

    lax.fori_loop(0, seqs, one, 0)


def mix_kernel(z, a0, a1, a2, a3, wa, wb, tok, gain, middle, normed, act, mid):
    quarter = a0.shape[1] // 2
    for d, a in enumerate((a0, a1, a2, a3)):
        at = pl.multiple_of(lax.rem(z[0] + d, 4) * quarter, quarter)
        act[0, :, pl.ds(at, quarter)] = a[:, :quarter]
        act[1, :, pl.ds(at, quarter)] = a[:, quarter:]
    inner = wa.shape[-1]
    square = jnp.zeros((tok.shape[0], 128), f32)
    for zl, y, at in k_blocks():
        one = mm_t(act[0], wa[zl, y].reshape(256, inner)).astype(bf16).astype(f32)
        two = mm_t(act[1], wb[zl, y].reshape(256, inner)).astype(bf16).astype(f32)
        m = (tok[:, at : at + 256].astype(f32) + (one + two)).astype(bf16)
        middle[:, at : at + 256] = m
        m = m.astype(f32)
        mid[:, at : at + 256] = m
        square = square + m[:, :128] * m[:, :128] + m[:, 128:] * m[:, 128:]
    width = tok.shape[1]
    scale = lax.rsqrt(jnp.sum(square, axis=-1, keepdims=True) * (1.0 / width) + norm_eps)
    normed[...] = (mid[...] * scale * gain[...]).astype(bf16)


def ffn_kernel(x, ga, gb, da, db, out):
    hidden = []
    for w in (ga, gb):
        both = times_rows(x, w)
        half = both.shape[1] // 2
        gate = both[:, :half]
        hidden.append((gate * jax.nn.sigmoid(gate) * both[:, half:]).astype(bf16))
    inner = da.shape[-1]
    for zl, y, at in k_blocks():
        part = mm_t(hidden[0], da[zl, y].reshape(256, inner))
        part = part + mm_t(hidden[1], db[zl, y].reshape(256, inner))
        out[:, at : at + 256] = part.astype(out.dtype)


def layer(
    tokens,
    mix_gain,
    value_weight,
    gate_weight,
    conv_taps,
    head_gain,
    out_weight,
    ffn_gain,
    ffn_gate_weight,
    ffn_up_weight,
    down_weight,
):
    rows, _, width = tokens.shape
    zh, zl = lax.axis_index("zh"), lax.axis_index("zl")
    z = 2 * zh + zl
    tp = lax.axis_index("tp")
    ch = value_weight.shape[1] // 4

    def quarter(weight, of):
        size = weight.shape[1] // 4
        return lax.dynamic_slice_in_dim(weight, of * size, size, axis=1)

    def mine_theirs(*weights):
        return tuple(
            jnp.concatenate([quarter(w, of) for w in weights], axis=1) for of in (z, 2 * zh + 1 - zl)
        )

    def paired(mine, theirs):
        got = swap(theirs, "zl")
        return jnp.where(zl == 0, mine, got), jnp.where(zl == 0, got, mine)

    tok2 = tokens.reshape(rows, width)
    vg_mine, vg_theirs = mine_theirs(value_weight, gate_weight)
    vg_cols = vg_mine.shape[1]
    out_mine = out_weight.T
    out_cols = out_mine.shape[1]
    pair = paired(jnp.concatenate([vg_mine, out_mine], axis=1), jnp.concatenate([vg_theirs, out_mine], axis=1))
    vg, outw = ordered(*two_ways(pair), (vg_cols, out_cols))

    xs = ring(tok2, Z)

    gu_mine, gu_theirs = mine_theirs(ffn_gate_weight, ffn_up_weight)
    dn_mine, dn_theirs = mine_theirs(down_weight.T)
    gu_cols, dn_cols = gu_mine.shape[1], dn_mine.shape[1]
    pair = paired(jnp.concatenate([gu_mine, dn_mine], axis=1), jnp.concatenate([gu_theirs, dn_theirs], axis=1))
    gu, down = ordered(*two_ways(pair), (gu_cols, dn_cols))

    small = jnp.concatenate([conv_taps, head_gain[None]], axis=0)
    small = lax.dynamic_slice_in_dim(small, z * ch, ch, axis=1)
    small = jnp.concatenate([small, swap(small, "tp")], axis=1)

    (glu,) = whole_call(
        glu_kernel,
        [((4, rows, 2 * ch), bf16)],
        [*xs, mix_gain.reshape(1, width), vg, swap(vg, "tp")],
        flops=4 * rows * width * 4 * ch * 2,
    )
    edge = lax.dynamic_slice_in_dim(glu, jnp.where(tp == 0, rows - HALO, 0), HALO, axis=1)
    edge = swap(edge, "tp")
    (activated,) = whole_call(
        conv_kernel,
        [((4, rows, 2 * ch), bf16)],
        [tp.astype(jnp.int32).reshape(1), glu, edge, small],
        scratch=[pltpu.VMEM((rows + 2 * HALO, 2 * ch), f32)],
        flops=4 * rows * 2 * ch * 64,
    )
    back = {0: activated[0], **{d: shift_z(activated[1 + i], -d) for i, d in enumerate(SHIFTS)}}
    middle, normed_ffn = whole_call(
        mix_kernel,
        [((rows, width), bf16), ((rows, width), bf16)],
        [
            z.astype(jnp.int32).reshape(1),
            *[back[d] for d in range(4)],
            outw,
            swap(outw, "tp"),
            tok2,
            ffn_gain.reshape(1, width),
        ],
        scratch=[pltpu.VMEM((2, rows, 4 * ch), bf16), pltpu.VMEM((rows, width), f32)],
        flops=rows * width * 8 * ch * 2,
    )
    gu_other, down_other = swap(gu, "tp"), swap(down, "tp")
    far = [shift_z(normed_ffn, d) for d in SHIFTS]
    ff_flops = rows * width * gu_cols * 6

    def piece(x, kind):
        (out,) = whole_call(ffn_kernel, [((rows, width), kind)], [x, gu, gu_other, down, down_other], flops=ff_flops)
        return out

    returned = [shift_z(piece(x, bf16), -d) for x, d in zip(far, SHIFTS)]
    fed = piece(normed_ffn, f32)
    for part in returned:
        fed = fed + part.astype(f32)
    return (middle.astype(f32) + fed).astype(bf16).reshape(tokens.shape)


def solution(mesh):
    fine = Mesh(mesh.devices.reshape(2, 2, 4, 4, 2), ("zh", "zl", "y", "x", "tp"))
    wide = P(FS, "tp")
    seqs = P("tp", ("zh", "zl", "y", "x"), None)
    placed = (
        seqs,
        P(),
        wide,
        wide,
        P(None, "tp"),
        P("tp"),
        P("tp", FS),
        P(),
        wide,
        wide,
        P("tp", FS),
    )
    return jax.shard_map(layer, mesh=fine, in_specs=placed, out_specs=seqs, check_vma=False)
```

profile of v0, /device:TPU:1, one launch (start us, length us, event | category | flops | bytes accessed | tf_op | source)
XLA Modules:
  0.0 217.2 jit_solution(941388302591918587)
XLA Ops:
  7.9 2.7 %collective-permute-start.26 = (bf16[64,1152]{1,0:T(8,128)(2,1)S(1)}, bf16[64,1152]{1,0:T(8,128)(2,1)S(1)}, u32[]{:S(2)}, u32[]{:S(2)}) collective-permute-start(bf16[64,1152]{1,0:T(8,128)(2,1)S(1)} %get-tuple-element.18), channel_id=1, source_target_pairs={{0,4},{2,6},{4,0},{6,2},{1,5},{3,7},{5,1},{7,3},{8,12},{10,14},{12... | collective-permute-start | bytes 442376 | tf_op jit(solution)/shard_map/ppermute | solution.py:32
  16.4 2.9 %collective-permute-done.24 = bf16[64,1152]{1,0:T(8,128)(2,1)S(1)} collective-permute-done((bf16[64,1152]{1,0:T(8,128)(2,1)S(1)}, bf16[64,1152]{1,0:T(8,128)(2,1)S(1)}, u32[]{:S(2)}, u32[]{:S(2)}) %collective-permute-start.24) | collective-permute-done | bytes 147488 | tf_op jit(solution)/shard_map/ppermute | solution.py:32
  26.0 8.9 %collective-permute-done.12 = bf16[64,768]{1,0:T(8,128)(2,1)} collective-permute-done((bf16[64,768]{1,0:T(8,128)(2,1)S(1)}, bf16[64,768]{1,0:T(8,128)(2,1)}, u32[]{:S(2)}, u32[]{:S(2)}) %collective-permute-start.12) | collective-permute-done | bytes 98336 | tf_op jit(solution)/shard_map/ppermute | solution.py:32
  34.9 3.1 %collective-permute-done.32 = bf16[64,1152]{1,0:T(8,128)(2,1)S(1)} collective-permute-done((bf16[64,1152]{1,0:T(8,128)(2,1)S(1)}, bf16[64,1152]{1,0:T(8,128)(2,1)S(1)}, u32[]{:S(2)}, u32[]{:S(2)}) %collective-permute-start.32) | collective-permute-done | bytes 147488 | tf_op jit(solution)/shard_map/ppermute | solution.py:32
  40.3 7.4 %collective-permute-done.11 = bf16[64,768]{1,0:T(8,128)(2,1)S(1)} collective-permute-done((bf16[64,768]{1,0:T(8,128)(2,1)S(1)}, bf16[64,768]{1,0:T(8,128)(2,1)S(1)}, u32[]{:S(2)}, u32[]{:S(2)}) %collective-permute-start.11) | collective-permute-done | bytes 98336 | tf_op jit(solution)/shard_map/ppermute | solution.py:32
  58.5 3.6 %collective-permute-done.29.refs_3_ = bf16[4,64,1152]{2,1,0:T(8,128)(2,1)S(1)} collective-permute-done((bf16[4,64,1152]{2,1,0:T(8,128)(2,1)S(1)}, bf16[4,64,1152]{2,1,0:T(8,128)(2,1)S(1)}, u32[]{:S(2)}, u32[]{:S(2)}) %collective-permute-start.29) | collective-permute-done | bytes 589856 | tf_op jit(solution)/shard_map/ppermute | solution.py:32
  67.5 4.0 %collective-permute-start.15 = (bf16[4,64,768]{2,1,0:T(8,128)(2,1)S(1)}, bf16[4,64,768]{2,1,0:T(8,128)(2,1)S(1)}, u32[]{:S(2)}, u32[]{:S(2)}) collective-permute-start(bf16[4,64,768]{2,1,0:T(8,128)(2,1)S(1)} %pad_maximum_fusion.3.refs_4_), channel_id=1, source_target_pairs={{0,4},{2,6},{4,0},{6,2},{1,5},{3,7},{5,1},{7,3},{8,12},{10,14},{12... | collective-permute-start | bytes 1179656 | tf_op jit(solution)/shard_map/ppermute | solution.py:32
  71.5 5.0 %shard_map.113 = (bf16[2,4,4,64,768]{4,3,2,1,0:T(8,128)(2,1)}, bf16[2,4,4,64,384]{4,3,2,1,0:T(8,128)(2,1)}) custom-call(s32[2]{0:T(128)S(1)} %pad_add_fusion.at, bf16[4,64,1152]{2,1,0:T(8,128)(2,1)S(1)} %pad_maximum_fusion.refs_0_, bf16[4,64,1152]{2,1,0:T(8,128)(2,1)S(1)} %collective-permute-done.27.refs_1_, ...), custom_call_target="tpu_custom_call" | custom-call | flops 1073741824 | bytes 4194304 | tf_op jit(solution)/shard_map/pallas_call | solution.py:67
  76.5 20.3 %collective-permute-start.36 = (bf16[2,4,4,64,768]{4,3,2,1,0:T(8,128)(2,1)}, bf16[2,4,4,64,768]{4,3,2,1,0:T(8,128)(2,1)}, u32[]{:S(2)}, u32[]{:S(2)}) collective-permute-start(bf16[2,4,4,64,768]{4,3,2,1,0:T(8,128)(2,1)} %get-tuple-element.15.ga), channel_id=1, source_target_pairs={{0,1},{1,0},{2,3},{3,2},{4,5},{5,4},{6,7},{7,6},{8,9},{9,8},{10,11... | collective-permute-start | bytes 9437192 | tf_op jit(solution)/shard_map/ppermute | solution.py:22
  96.8 4.2 %shard_map.109 = (bf16[2,4,4,64,256]{4,3,2,1,0:T(8,128)(2,1)}, bf16[2,4,4,64,512]{4,3,2,1,0:T(8,128)(2,1)}) custom-call(s32[2]{0:T(128)S(1)} %pad_add_fusion.at, bf16[4,64,768]{2,1,0:T(8,128)(2,1)} %pad_maximum_fusion.2.refs_0_, bf16[4,64,768]{2,1,0:T(8,128)(2,1)S(1)} %copy-done.9, bf16[4,64,768]{2,1,0:T(8,128)(2,1)} %collective-permute-done.8.refs_2_, ...), custom_call_target="tpu_custom_call" | custom-call | flops 1073741824 | bytes 4194304 | tf_op jit(solution)/shard_map/pallas_call | solution.py:67
  102.7 7.8 %collective-permute-start = (bf16[128,2048]{1,0:T(8,128)(2,1)}, bf16[128,2048]{1,0:T(8,128)(2,1)S(1)}, u32[]{:S(2)}, u32[]{:S(2)}) collective-permute-start(bf16[128,2048]{1,0:T(8,128)(2,1)} %bitcast.2.x0.tok), channel_id=1, source_target_pairs={{0,32},{32,64},{64,96},{96,0},{1,33},{33,65},{65,97},{97,1},{2,34}... | collective-permute-start | bytes 1572872 | tf_op jit(solution)/shard_map/ppermute | solution.py:32
  113.0 12.1 %collective-permute-done.x1 = bf16[128,2048]{1,0:T(8,128)(2,1)S(1)} collective-permute-done((bf16[128,2048]{1,0:T(8,128)(2,1)}, bf16[128,2048]{1,0:T(8,128)(2,1)S(1)}, u32[]{:S(2)}, u32[]{:S(2)}) %collective-permute-start) | collective-permute-done | bytes 524320 | tf_op jit(solution)/shard_map/ppermute | solution.py:32
  128.2 12.3 %collective-permute-done.2.x3 = bf16[128,2048]{1,0:T(8,128)(2,1)} collective-permute-done((bf16[128,2048]{1,0:T(8,128)(2,1)}, bf16[128,2048]{1,0:T(8,128)(2,1)}, u32[]{:S(2)}, u32[]{:S(2)}) %collective-permute-start.2) | collective-permute-done | bytes 524320 | tf_op jit(solution)/shard_map/ppermute | solution.py:32
  144.1 3.6 %shard_map.110.glu = bf16[4,128,256]{2,1,0:T(8,128)(2,1)S(1)} custom-call(bf16[128,2048]{1,0:T(8,128)(2,1)} %bitcast.2.x0.tok, bf16[128,2048]{1,0:T(8,128)(2,1)S(1)} %copy-done.3, bf16[128,2048]{1,0:T(8,128)(2,1)S(1)} %copy-done.5, bf16[128,2048]{1,0:T(8,128)(2,1)} %collective-permute-done.2.x3, f32[1,2048]{1,0:T(1,128)S(1)} %bitcast.39, ...), custom_call_target="tpu_custom_call" | custom-call | flops 1073741824 | bytes 1048576 | tf_op jit(solution)/shard_map/pallas_call | solution.py:92
  149.0 3.8 %shard_map.111 = bf16[4,128,256]{2,1,0:T(8,128)(2,1)S(1)} custom-call(s32[1]{0:T(128)} %bitcast.1.tp, bf16[4,128,256]{2,1,0:T(8,128)(2,1)S(1)} %shard_map.110.glu, bf16[4,16,256]{2,1,0:T(8,128)(2,1)S(1)} %collective-permute-done.17.edge, f32[32,256]{1,0:T(8,128)S(1)} %pad_maximum_fusion.8.small), custom_call_target="tpu_custom_call" | custom-call | flops 8388608 | bytes 1048576 | tf_op jit(solution)/shard_map/pallas_call | solution.py:92
  160.8 3.3 %shard_map.112 = (bf16[128,2048]{1,0:T(8,128)(2,1)S(1)}, bf16[128,2048]{1,0:T(8,128)(2,1)S(1)}) custom-call(s32[1]{0:T(128)} %bitcast.z, bf16[128,256]{1,0:T(8,128)(2,1)S(1)} %get-tuple-element.22.a0, bf16[128,256]{1,0:T(8,128)(2,1)S(1)} %collective-permute-done.19.a1, bf16[128,256]{1,0:T(8,128)(2,1)S(1)} %collective-permute-done.20.a2, ...), custom_call_target="tpu_custom_call" | custom-call | flops 536870912 | bytes 1048576 | tf_op jit(solution)/shard_map/pallas_call | solution.py:92
  166.2 10.2 %collective-permute-done.42.x = bf16[128,2048]{1,0:T(8,128)(2,1)S(1)} collective-permute-done((bf16[128,2048]{1,0:T(8,128)(2,1)S(1)}, bf16[128,2048]{1,0:T(8,128)(2,1)S(1)}, u32[]{:S(2)}, u32[]{:S(2)}) %collective-permute-start.42) | collective-permute-done | bytes 524320 | tf_op jit(solution)/shard_map/ppermute | solution.py:26
  176.5 5.3 %shard_map.117 = bf16[128,2048]{1,0:T(8,128)(2,1)S(1)} custom-call(bf16[128,2048]{1,0:T(8,128)(2,1)S(1)} %collective-permute-done.42.x, bf16[2,4,4,64,768]{4,3,2,1,0:T(8,128)(2,1)} %get-tuple-element.15.ga, bf16[2,4,4,64,768]{4,3,2,1,0:T(8,128)(2,1)} %collective-permute-done.36.gb, bf16[2,4,4,64,384]{4,3,2,1,0:T(8,128)(2,1)S(1)} %copy-done, ...), custom_call_target="tpu_custom_call" | custom-call | flops 1207959552 | bytes 1048576 | tf_op jit(solution)/shard_map/pallas_call | solution.py:92
  182.7 8.4 %collective-permute-done.40.x = bf16[128,2048]{1,0:T(8,128)(2,1)S(1)} collective-permute-done((bf16[128,2048]{1,0:T(8,128)(2,1)S(1)}, bf16[128,2048]{1,0:T(8,128)(2,1)S(1)}, u32[]{:S(2)}, u32[]{:S(2)}) %collective-permute-start.40) | collective-permute-done | bytes 524320 | tf_op jit(solution)/shard_map/ppermute | solution.py:26
  191.1 5.3 %shard_map.116 = bf16[128,2048]{1,0:T(8,128)(2,1)S(1)} custom-call(bf16[128,2048]{1,0:T(8,128)(2,1)S(1)} %collective-permute-done.40.x, bf16[2,4,4,64,768]{4,3,2,1,0:T(8,128)(2,1)} %get-tuple-element.15.ga, bf16[2,4,4,64,768]{4,3,2,1,0:T(8,128)(2,1)} %collective-permute-done.36.gb, bf16[2,4,4,64,384]{4,3,2,1,0:T(8,128)(2,1)S(1)} %copy-done, ...), custom_call_target="tpu_custom_call" | custom-call | flops 1207959552 | bytes 1048576 | tf_op jit(solution)/shard_map/pallas_call | solution.py:92
  198.0 5.3 %shard_map.115 = bf16[128,2048]{1,0:T(8,128)(2,1)S(1)} custom-call(bf16[128,2048]{1,0:T(8,128)(2,1)S(1)} %collective-permute-done.38.x, bf16[2,4,4,64,768]{4,3,2,1,0:T(8,128)(2,1)} %get-tuple-element.15.ga, bf16[2,4,4,64,768]{4,3,2,1,0:T(8,128)(2,1)} %collective-permute-done.36.gb, bf16[2,4,4,64,384]{4,3,2,1,0:T(8,128)(2,1)S(1)} %copy-done, ...), custom_call_target="tpu_custom_call" | custom-call | flops 1207959552 | bytes 1048576 | tf_op jit(solution)/shard_map/pallas_call | solution.py:92
  203.2 2.7 %collective-permute-start.39 = (bf16[128,2048]{1,0:T(8,128)(2,1)S(1)}, bf16[128,2048]{1,0:T(8,128)(2,1)S(1)}, u32[]{:S(2)}, u32[]{:S(2)}) collective-permute-start(bf16[128,2048]{1,0:T(8,128)(2,1)S(1)} %shard_map.115), channel_id=1, source_target_pairs={{0,96},{32,0},{64,32},{96,64},{1,97},{33,1},{65,33},{97,65},{2,98}... | collective-permute-start | bytes 1572872 | tf_op jit(solution)/shard_map/ppermute | solution.py:26
  205.9 5.3 %shard_map.114 = f32[128,2048]{1,0:T(8,128)S(1)} custom-call(bf16[128,2048]{1,0:T(8,128)(2,1)S(1)} %get-tuple-element.14.x, bf16[2,4,4,64,768]{4,3,2,1,0:T(8,128)(2,1)} %get-tuple-element.15.ga, bf16[2,4,4,64,768]{4,3,2,1,0:T(8,128)(2,1)} %collective-permute-done.36.gb, bf16[2,4,4,64,384]{4,3,2,1,0:T(8,128)(2,1)S(1)} %copy-done, ...), custom_call_target="tpu_custom_call" | custom-call | flops 1207959552 | bytes 1048576 | tf_op jit(solution)/shard_map/pallas_call | solution.py:92
  212.3 3.7 %collective-permute-done.39 = bf16[128,2048]{1,0:T(8,128)(2,1)S(1)} collective-permute-done((bf16[128,2048]{1,0:T(8,128)(2,1)S(1)}, bf16[128,2048]{1,0:T(8,128)(2,1)S(1)}, u32[]{:S(2)}, u32[]{:S(2)}) %collective-permute-start.39) | collective-permute-done | bytes 524320 | tf_op jit(solution)/shard_map/ppermute | solution.py:26
  (120 shorter events, 65.8 us)
Async XLA Ops:
  19.3 34.9 %collective-permute-start.27 = (bf16[4,64,1152]{2,1,0:T(8,128)(2,1)S(1)}, bf16[4,64,1152]{2,1,0:T(8,128)(2,1)S(1)}, u32[]{:S(2)}, u32[]{:S(2)}) collective-permute-start(bf16[4,64,1152]{2,1,0:T(8,128)(2,1)S(1)} %pad_maximum_fusion.refs_0_), channel_id=1, source_target_pairs={{0,8},{8,16},{16,24},{24,0},{1,9},{9,17},{17,25},{25,1},{2,10},{10... | collective-permute-start | bytes 1769480 | tf_op jit(solution)/shard_map/ppermute | solution.py:32
  20.7 14.2 %collective-permute-start.12 = (bf16[64,768]{1,0:T(8,128)(2,1)S(1)}, bf16[64,768]{1,0:T(8,128)(2,1)}, u32[]{:S(2)}, u32[]{:S(2)}) collective-permute-start(bf16[64,768]{1,0:T(8,128)(2,1)S(1)} %get-tuple-element.29), channel_id=1, source_target_pairs={{0,16},{8,24},{16,0},{24,8},{1,17},{9,25},{17,1},{25,9},{2,18},{10... | collective-permute-start | bytes 294920 | tf_op jit(solution)/shard_map/ppermute | solution.py:32
  23.3 14.7 %collective-permute-start.32 = (bf16[64,1152]{1,0:T(8,128)(2,1)S(1)}, bf16[64,1152]{1,0:T(8,128)(2,1)S(1)}, u32[]{:S(2)}, u32[]{:S(2)}) collective-permute-start(bf16[64,1152]{1,0:T(8,128)(2,1)S(1)} %get-tuple-element.17), channel_id=1, source_target_pairs={{0,16},{8,24},{16,0},{24,8},{1,17},{9,25},{17,1},{25,9},{2,18},{10... | collective-permute-start | bytes 442376 | tf_op jit(solution)/shard_map/ppermute | solution.py:32
  23.7 14.3 %collective-permute-start.31 = (bf16[64,1152]{1,0:T(8,128)(2,1)S(1)}, bf16[64,1152]{1,0:T(8,128)(2,1)S(1)}, u32[]{:S(2)}, u32[]{:S(2)}) collective-permute-start(bf16[64,1152]{1,0:T(8,128)(2,1)S(1)} %get-tuple-element.17), channel_id=1, source_target_pairs={{0,24},{8,0},{16,8},{24,16},{1,25},{9,1},{17,9},{25,17},{2,26},{10... | collective-permute-start | bytes 442376 | tf_op jit(solution)/shard_map/ppermute | solution.py:32
  25.2 13.4 %collective-permute-start.30 = (bf16[64,1152]{1,0:T(8,128)(2,1)S(1)}, bf16[64,1152]{1,0:T(8,128)(2,1)S(1)}, u32[]{:S(2)}, u32[]{:S(2)}) collective-permute-start(bf16[64,1152]{1,0:T(8,128)(2,1)S(1)} %get-tuple-element.17), channel_id=1, source_target_pairs={{0,8},{8,16},{16,24},{24,0},{1,9},{9,17},{17,25},{25,1},{2,10},{10... | collective-permute-start | bytes 442376 | tf_op jit(solution)/shard_map/ppermute | solution.py:32
  34.9 17.9 %collective-permute-start.7 = (bf16[4,64,768]{2,1,0:T(8,128)(2,1)}, bf16[4,64,768]{2,1,0:T(8,128)(2,1)S(1)}, u32[]{:S(2)}, u32[]{:S(2)}) collective-permute-start(bf16[4,64,768]{2,1,0:T(8,128)(2,1)} %pad_maximum_fusion.2.refs_0_), channel_id=1, source_target_pairs={{0,8},{8,16},{16,24},{24,0},{1,9},{9,17},{17,25},{25,1},{2,10},{10... | collective-permute-start | bytes 1179656 | tf_op jit(solution)/shard_map/ppermute | solution.py:32
  38.0 17.9 %collective-permute-start.28 = (bf16[4,64,1152]{2,1,0:T(8,128)(2,1)S(1)}, bf16[4,64,1152]{2,1,0:T(8,128)(2,1)S(1)}, u32[]{:S(2)}, u32[]{:S(2)}) collective-permute-start(bf16[4,64,1152]{2,1,0:T(8,128)(2,1)S(1)} %pad_maximum_fusion.refs_0_), channel_id=1, source_target_pairs={{0,24},{8,0},{16,8},{24,16},{1,25},{9,1},{17,9},{25,17},{2,26},{10... | collective-permute-start | bytes 1769480 | tf_op jit(solution)/shard_map/ppermute | solution.py:32
  47.8 14.4 %collective-permute-start.29 = (bf16[4,64,1152]{2,1,0:T(8,128)(2,1)S(1)}, bf16[4,64,1152]{2,1,0:T(8,128)(2,1)S(1)}, u32[]{:S(2)}, u32[]{:S(2)}) collective-permute-start(bf16[4,64,1152]{2,1,0:T(8,128)(2,1)S(1)} %pad_maximum_fusion.refs_0_), channel_id=1, source_target_pairs={{0,16},{8,24},{16,0},{24,8},{1,17},{9,25},{17,1},{25,9},{2,18},{10... | collective-permute-start | bytes 1769480 | tf_op jit(solution)/shard_map/ppermute | solution.py:32
  55.9 20.6 %collective-permute-start.8 = (bf16[4,64,768]{2,1,0:T(8,128)(2,1)}, bf16[4,64,768]{2,1,0:T(8,128)(2,1)}, u32[]{:S(2)}, u32[]{:S(2)}) collective-permute-start(bf16[4,64,768]{2,1,0:T(8,128)(2,1)} %pad_maximum_fusion.2.refs_0_), channel_id=1, source_target_pairs={{0,24},{8,0},{16,8},{24,16},{1,25},{9,1},{17,9},{25,17},{2,26},{10... | collective-permute-start | bytes 1179656 | tf_op jit(solution)/shard_map/ppermute | solution.py:32
  62.2 34.6 %collective-permute-start.9 = (bf16[4,64,768]{2,1,0:T(8,128)(2,1)}, bf16[4,64,768]{2,1,0:T(8,128)(2,1)S(1)}, u32[]{:S(2)}, u32[]{:S(2)}) collective-permute-start(bf16[4,64,768]{2,1,0:T(8,128)(2,1)} %pad_maximum_fusion.2.refs_0_), channel_id=1, source_target_pairs={{0,16},{8,24},{16,0},{24,8},{1,17},{9,25},{17,1},{25,9},{2,18},{10... | collective-permute-start | bytes 1179656 | tf_op jit(solution)/shard_map/ppermute | solution.py:32
  62.6 34.1 %collective-permute-start.13 = (bf16[4,64,768]{2,1,0:T(8,128)(2,1)S(1)}, bf16[4,64,768]{2,1,0:T(8,128)(2,1)S(1)}, u32[]{:S(2)}, u32[]{:S(2)}) collective-permute-start(bf16[4,64,768]{2,1,0:T(8,128)(2,1)S(1)} %pad_maximum_fusion.3.refs_4_), channel_id=1, source_target_pairs={{0,2},{2,4},{4,6},{6,0},{1,3},{3,5},{5,7},{7,1},{8,10},{10,12},{12... | collective-permute-start | bytes 1179656 | tf_op jit(solution)/shard_map/ppermute | solution.py:32
  63.2 33.5 %collective-permute-start.14 = (bf16[4,64,768]{2,1,0:T(8,128)(2,1)S(1)}, bf16[4,64,768]{2,1,0:T(8,128)(2,1)S(1)}, u32[]{:S(2)}, u32[]{:S(2)}) collective-permute-start(bf16[4,64,768]{2,1,0:T(8,128)(2,1)S(1)} %pad_maximum_fusion.3.refs_4_), channel_id=1, source_target_pairs={{0,6},{2,0},{4,2},{6,4},{1,7},{3,1},{5,3},{7,5},{8,14},{10,8},{12,... | collective-permute-start | bytes 1179656 | tf_op jit(solution)/shard_map/ppermute | solution.py:32
  67.5 29.3 %collective-permute-start.15 = (bf16[4,64,768]{2,1,0:T(8,128)(2,1)S(1)}, bf16[4,64,768]{2,1,0:T(8,128)(2,1)S(1)}, u32[]{:S(2)}, u32[]{:S(2)}) collective-permute-start(bf16[4,64,768]{2,1,0:T(8,128)(2,1)S(1)} %pad_maximum_fusion.3.refs_4_), channel_id=1, source_target_pairs={{0,4},{2,6},{4,0},{6,2},{1,5},{3,7},{5,1},{7,3},{8,12},{10,14},{12... | collective-permute-start | bytes 1179656 | tf_op jit(solution)/shard_map/ppermute | solution.py:32
  76.5 99.9 %collective-permute-start.36 = (bf16[2,4,4,64,768]{4,3,2,1,0:T(8,128)(2,1)}, bf16[2,4,4,64,768]{4,3,2,1,0:T(8,128)(2,1)}, u32[]{:S(2)}, u32[]{:S(2)}) collective-permute-start(bf16[2,4,4,64,768]{4,3,2,1,0:T(8,128)(2,1)} %get-tuple-element.15.ga), channel_id=1, source_target_pairs={{0,1},{1,0},{2,3},{3,2},{4,5},{5,4},{6,7},{7,6},{8,9},{9,8},{10,11... | collective-permute-start | bytes 9437192 | tf_op jit(solution)/shard_map/ppermute | solution.py:22
  101.0 59.8 %collective-permute-start.22 = (bf16[2,4,4,64,512]{4,3,2,1,0:T(8,128)(2,1)}, bf16[2,4,4,64,512]{4,3,2,1,0:T(8,128)(2,1)}, u32[]{:S(2)}, u32[]{:S(2)}) collective-permute-start(bf16[2,4,4,64,512]{4,3,2,1,0:T(8,128)(2,1)} %get-tuple-element.12.wa), channel_id=1, source_target_pairs={{0,1},{1,0},{2,3},{3,2},{4,5},{5,4},{6,7},{7,6},{8,9},{9,8},{10,11... | collective-permute-start | bytes 6291464 | tf_op jit(solution)/shard_map/ppermute | solution.py:22
  102.7 22.3 %collective-permute-start = (bf16[128,2048]{1,0:T(8,128)(2,1)}, bf16[128,2048]{1,0:T(8,128)(2,1)S(1)}, u32[]{:S(2)}, u32[]{:S(2)}) collective-permute-start(bf16[128,2048]{1,0:T(8,128)(2,1)} %bitcast.2.x0.tok), channel_id=1, source_target_pairs={{0,32},{32,64},{64,96},{96,0},{1,33},{33,65},{65,97},{97,1},{2,34}... | collective-permute-start | bytes 1572872 | tf_op jit(solution)/shard_map/ppermute | solution.py:32
  110.5 31.5 %collective-permute-start.16 = (bf16[2,4,4,64,256]{4,3,2,1,0:T(8,128)(2,1)}, bf16[2,4,4,64,256]{4,3,2,1,0:T(8,128)(2,1)}, u32[]{:S(2)}, u32[]{:S(2)}) collective-permute-start(bf16[2,4,4,64,256]{4,3,2,1,0:T(8,128)(2,1)} %get-tuple-element.11.wa), channel_id=1, source_target_pairs={{0,1},{1,0},{2,3},{3,2},{4,5},{5,4},{6,7},{7,6},{8,9},{9,8},{10,11... | collective-permute-start | bytes 3145736 | tf_op jit(solution)/shard_map/ppermute | solution.py:22
  110.9 15.3 %collective-permute-start.1 = (bf16[128,2048]{1,0:T(8,128)(2,1)}, bf16[128,2048]{1,0:T(8,128)(2,1)S(1)}, u32[]{:S(2)}, u32[]{:S(2)}) collective-permute-start(bf16[128,2048]{1,0:T(8,128)(2,1)} %bitcast.2.x0.tok), channel_id=1, source_target_pairs={{0,96},{32,0},{64,32},{96,64},{1,97},{33,1},{65,33},{97,65},{2,98}... | collective-permute-start | bytes 1572872 | tf_op jit(solution)/shard_map/ppermute | solution.py:32
  125.9 14.6 %collective-permute-start.2 = (bf16[128,2048]{1,0:T(8,128)(2,1)}, bf16[128,2048]{1,0:T(8,128)(2,1)}, u32[]{:S(2)}, u32[]{:S(2)}) collective-permute-start(bf16[128,2048]{1,0:T(8,128)(2,1)} %bitcast.2.x0.tok), channel_id=1, source_target_pairs={{0,64},{32,96},{64,0},{96,32},{1,65},{33,97},{65,1},{97,33},{2,66}... | collective-permute-start | bytes 1572872 | tf_op jit(solution)/shard_map/ppermute | solution.py:32
  126.9 39.3 %collective-permute-start.37 = (bf16[2,4,4,64,384]{4,3,2,1,0:T(8,128)(2,1)S(1)}, bf16[2,4,4,64,384]{4,3,2,1,0:T(8,128)(2,1)S(1)}, u32[]{:S(2)}, u32[]{:S(2)}) collective-permute-start(bf16[2,4,4,64,384]{4,3,2,1,0:T(8,128)(2,1)S(1)} %copy-done), channel_id=1, source_target_pairs={{0,1},{1,0},{2,3},{3,2},{4,5},{5,4},{6,7},{7,6},{8,9},{9,8},{10,11... | collective-permute-start | bytes 4718600 | tf_op jit(solution)/shard_map/ppermute | solution.py:22
  164.8 26.3 %collective-permute-start.40 = (bf16[128,2048]{1,0:T(8,128)(2,1)S(1)}, bf16[128,2048]{1,0:T(8,128)(2,1)S(1)}, u32[]{:S(2)}, u32[]{:S(2)}) collective-permute-start(bf16[128,2048]{1,0:T(8,128)(2,1)S(1)} %get-tuple-element.14.x), channel_id=1, source_target_pairs={{0,96},{32,0},{64,32},{96,64},{1,97},{33,1},{65,33},{97,65},{2,98}... | collective-permute-start | bytes 1572872 | tf_op jit(solution)/shard_map/ppermute | solution.py:26
  165.7 32.3 %collective-permute-start.38 = (bf16[128,2048]{1,0:T(8,128)(2,1)S(1)}, bf16[128,2048]{1,0:T(8,128)(2,1)S(1)}, u32[]{:S(2)}, u32[]{:S(2)}) collective-permute-start(bf16[128,2048]{1,0:T(8,128)(2,1)S(1)} %get-tuple-element.14.x), channel_id=1, source_target_pairs={{0,32},{32,64},{64,96},{96,0},{1,33},{33,65},{65,97},{97,1},{2,34}... | collective-permute-start | bytes 1572872 | tf_op jit(solution)/shard_map/ppermute | solution.py:26
  181.7 29.5 %collective-permute-start.43 = (bf16[128,2048]{1,0:T(8,128)(2,1)S(1)}, bf16[128,2048]{1,0:T(8,128)(2,1)S(1)}, u32[]{:S(2)}, u32[]{:S(2)}) collective-permute-start(bf16[128,2048]{1,0:T(8,128)(2,1)S(1)} %shard_map.117), channel_id=1, source_target_pairs={{0,64},{32,96},{64,0},{96,32},{1,65},{33,97},{65,1},{97,33},{2,66}... | collective-permute-start | bytes 1572872 | tf_op jit(solution)/shard_map/ppermute | solution.py:26
  196.4 15.9 %collective-permute-start.41 = (bf16[128,2048]{1,0:T(8,128)(2,1)S(1)}, bf16[128,2048]{1,0:T(8,128)(2,1)S(1)}, u32[]{:S(2)}, u32[]{:S(2)}) collective-permute-start(bf16[128,2048]{1,0:T(8,128)(2,1)S(1)} %shard_map.116), channel_id=1, source_target_pairs={{0,32},{32,64},{64,96},{96,0},{1,33},{33,65},{65,97},{97,1},{2,34}... | collective-permute-start | bytes 1572872 | tf_op jit(solution)/shard_map/ppermute | solution.py:26
  (35 other events, 517.7 us)
where the time goes:
time: 219 us; the launch traced here: 217 us
  waiting for transfers between devices  88.5 us (40%)
  starting transfers between devices  75.2 us (34%)
  Pallas kernels  41 us (19%)
  local copies, waits for them, and re-layouts  6.99 us (3%)
  other arithmetic  5.2 us (2%)
    ppermute x27, waiting for transfers between devices, ring(): got.append(lax.ppermute(value, axis, [(i, (i + d) % 4) for i in range(4)]))  55.4 us
    ppermute x27, starting transfers between devices, ring(): got.append(lax.ppermute(value, axis, [(i, (i + d) % 4) for i in range(4)]))  38.8 us
    pallas_call x7, Pallas kernels, whole_call(): pl.pallas_call(kernel, out_shape=[jax.ShapeDtypeStruct(s, d) for s, d in...  31.8 us
    ppermute x9, waiting for transfers between devices, shift_z(): return lax.ppermute(value, Z, [(i, (i + by) % 4) for i in range(4)])  30.1 us
    ppermute x8, starting transfers between devices, swap(): return lax.ppermute(value, axis, [(0, 1), (1, 0)])  27.9 us
    pallas_call x2, Pallas kernels, ordered(): pl.pallas_call(kernel, out_shape=[jax.ShapeDtypeStruct((2, 4, 4, 64, w),...  9.14 us
    ppermute x9, starting transfers between devices, shift_z(): return lax.ppermute(value, Z, [(i, (i + by) % 4) for i in range(4)])  8.58 us
    unnamed x30, local copies, waits for them, and re-layouts  4.45 us
  transfers between devices with their start and end apart: 44, of which 19 were waited for; matrix products, arithmetic and copies ran while one was open for 2% of the time, Pallas kernels for 19%

commit v1 on v0

--- a/solution.py
+++ b/solution.py
@@ -15,7 +15,7 @@
 SHIFTS = (1, 3, 2)
 f32 = jnp.float32
 bf16 = jnp.bfloat16
-VMEM_LIMIT = 48 * 1024 * 1024
+VMEM_LIMIT = 20 * 1024 * 1024
 
 
 def swap(value, axis):
@@ -33,46 +33,27 @@
     return got
 
 
-def two_ways(pair):
-    along_x = jnp.stack(ring(pair[0], "x"))
-    along_y = jnp.stack(ring(pair[1], "y"))
-    return ring(along_x, "y"), ring(along_y, "x")
-
-
-def ordered(first, second, widths):
+def ordered(groups, widths):
     offs = (0, *SHIFTS)
-    me = jnp.stack([lax.axis_index("y"), lax.axis_index("x")]).astype(jnp.int32)
+    me = jnp.stack([lax.axis_index(a) for a in ("y", "x", "zl")]).astype(jnp.int32)
     n = len(widths)
+    pieces = [p for first, second in groups for p in (*first, *second)]
 
     def kernel(at, *refs):
-        src, out, sem = refs[:8], refs[8 : 8 + n], refs[-1]
-        copies = []
-        for jy in range(4):
-            y = lax.rem(at[0] + 4 - offs[jy], 4)
-            for jx in range(4):
-                x = lax.rem(at[1] + 4 - offs[jx], 4)
-                for zl, ref in ((0, src[jy].at[jx]), (1, src[4 + jx].at[jy])):
-                    start = 0
-                    for k, w in enumerate(widths):
-                        copies.append(
-                            pltpu.make_async_copy(
-                                ref.at[:, start : start + w], out[k].at[zl, y, x], sem.at[len(copies)]
-                            )
-                        )
-                        copies[-1].start()
-                        start += w
-        for copy in copies:
-            copy.wait()
-
-    return pl.pallas_call(
-        kernel,
-        out_shape=[jax.ShapeDtypeStruct((2, 4, 4, 64, w), bf16) for w in widths],
-        in_specs=[pl.BlockSpec(memory_space=pltpu.SMEM)] + [pl.BlockSpec(memory_space=pltpu.HBM)] * 8,
-        out_specs=[pl.BlockSpec(memory_space=pltpu.VMEM)] * n,
-        scratch_shapes=[pltpu.SemaphoreType.DMA((32 * n,))],
-        cost_estimate=pl.CostEstimate(flops=1 << 30, transcendentals=0, bytes_accessed=1 << 22),
-        compiler_params=pltpu.CompilerParams(vmem_limit_bytes=VMEM_LIMIT),
-    )(me, *first, *second)
+        for g in range(len(groups)):
+            src = refs[8 * g : 8 * g + 8]
+            out = refs[len(pieces) + n * g : len(pieces) + n * g + n]
+            for jy in range(4):
+                y = lax.rem(at[0] + 4 - offs[jy], 4)
+                for jx in range(4):
+                    x = lax.rem(at[1] + 4 - offs[jx], 4)
+                    for zl, block in ((at[2], src[jy].at[jx]), (1 - at[2], src[4 + jx].at[jy])):
+                        start = 0
+                        for k, w in enumerate(widths):
+                            out[k][zl, y, x] = block[:, start : start + w]
+                            start += w
+
+    return whole_call(kernel, [((2, 4, 4, 64, w), bf16) for _ in groups for w in widths], [me, *pieces], flops=1 << 30)
 
 
 def mm(a, b):
@@ -83,11 +64,8 @@
     return lax.dot_general(a, b, (((1,), (1,)), ((), ())), preferred_element_type=f32)
 
 
-def whole_call(kernel, outs, args, scratch=(), flops=0):
-    specs = [
-        pl.BlockSpec(memory_space=pltpu.SMEM) if a.dtype == jnp.int32 else pl.BlockSpec(memory_space=pltpu.VMEM)
-        for a in args
-    ]
+def whole_call(kernel, outs, args, scratch=(), flops=0, space=pltpu.VMEM):
+    specs = [pl.BlockSpec(memory_space=pltpu.SMEM if a.dtype == jnp.int32 else space) for a in args]
     out_specs = [pl.BlockSpec(memory_space=pltpu.VMEM) for _ in outs]
     return pl.pallas_call(
         kernel,
@@ -104,12 +82,8 @@
     return [(zl, y, zl * 1024 + y * 256) for zl in range(2) for y in range(4)]
 
 
-def times_rows(x, w_ref):
-    cols = w_ref.shape[-1]
-    acc = jnp.zeros((x.shape[0], cols), f32)
-    for zl, y, at in k_blocks():
-        acc = acc + mm(x[:, at : at + 256], w_ref[zl, y].reshape(256, cols))
-    return acc
+def rows_of(w, start=0, stop=None):
+    return w[..., start:stop].reshape(-1, (stop or w.shape[-1]) - start)
 
 
 def glu_kernel(x0, x1, x2, x3, gain, wa, wb, out):
@@ -118,7 +92,7 @@
         scale = lax.rsqrt(jnp.mean(rows * rows, axis=-1, keepdims=True) + norm_eps)
         normed = (rows * scale * gain[...]).astype(bf16)
         for j, w in enumerate((wa, wb)):
-            both = times_rows(normed, w)
+            both = mm(normed, rows_of(w))
             half = both.shape[1] // 2
             out[i, :, j * half : (j + 1) * half] = (both[:, :half] * jax.nn.sigmoid(both[:, half:])).astype(bf16)
 
@@ -129,7 +103,7 @@
     taps = small.shape[0] - 1
     left = jnp.where(tp[0] == 1, 1.0, 0.0).astype(f32)
     right = 1.0 - left
-    chunk = 32
+    chunk = rows
 
     def one(s, carry):
         near = edge[s].astype(f32)
@@ -176,18 +150,36 @@
     normed[...] = (mid[...] * scale * gain[...]).astype(bf16)
 
 
-def ffn_kernel(x, ga, gb, da, db, out):
-    hidden = []
-    for w in (ga, gb):
-        both = times_rows(x, w)
-        half = both.shape[1] // 2
-        gate = both[:, :half]
-        hidden.append((gate * jax.nn.sigmoid(gate) * both[:, half:]).astype(bf16))
-    inner = da.shape[-1]
-    for zl, y, at in k_blocks():
-        part = mm_t(hidden[0], da[zl, y].reshape(256, inner))
-        part = part + mm_t(hidden[1], db[zl, y].reshape(256, inner))
-        out[:, at : at + 256] = part.astype(out.dtype)
+def ffn_kernel(*refs):
+    *xs, wa, wb, out = refs
+    x = xs[0][...] if len(xs) == 1 else jnp.concatenate([part[...] for part in xs], axis=0)
+    ff = wa.shape[-1] // 3
+    part = None
+    for w in (wa, wb):
+        both = mm(x, rows_of(w, 0, 2 * ff))
+        gate = both[:, :ff]
+        hidden = (gate * jax.nn.sigmoid(gate) * both[:, ff:]).astype(bf16)
+        one = mm_t(hidden, rows_of(w, 2 * ff, 3 * ff))
+        part = one if part is None else part + one
+    out[...] = part.astype(out.dtype)
+
+
+def prep_kernel(at, value, gate, outw, ffn_gate, ffn_up, down, mine, theirs, sem):
+    copies = []
+    for which, out in enumerate((mine, theirs)):
+        start = 0
+        for w in (value, gate, outw, ffn_gate, ffn_up, down):
+            if w is outw:
+                size = w.shape[1]
+                src = w
+            else:
+                size = w.shape[1] // 4
+                src = w.at[:, pl.ds(pl.multiple_of(at[which] * size, 128), size)]
+            copies.append(pltpu.make_async_copy(src, out.at[:, start : start + size], sem.at[len(copies)]))
+            copies[-1].start()
+            start += size
+    for copy in copies:
+        copy.wait()
 
 
 def layer(
@@ -209,34 +201,36 @@
     tp = lax.axis_index("tp")
     ch = value_weight.shape[1] // 4
 
-    def quarter(weight, of):
-        size = weight.shape[1] // 4
-        return lax.dynamic_slice_in_dim(weight, of * size, size, axis=1)
-
-    def mine_theirs(*weights):
-        return tuple(
-            jnp.concatenate([quarter(w, of) for w in weights], axis=1) for of in (z, 2 * zh + 1 - zl)
-        )
-
-    def paired(mine, theirs):
-        got = swap(theirs, "zl")
-        return jnp.where(zl == 0, mine, got), jnp.where(zl == 0, got, mine)
-
     tok2 = tokens.reshape(rows, width)
-    vg_mine, vg_theirs = mine_theirs(value_weight, gate_weight)
-    vg_cols = vg_mine.shape[1]
-    out_mine = out_weight.T
-    out_cols = out_mine.shape[1]
-    pair = paired(jnp.concatenate([vg_mine, out_mine], axis=1), jnp.concatenate([vg_theirs, out_mine], axis=1))
-    vg, outw = ordered(*two_ways(pair), (vg_cols, out_cols))
-
+    vg_cols, out_cols = 2 * ch, out_weight.shape[0]
+    gu_cols, dn_cols = ffn_gate_weight.shape[1] // 2, down_weight.shape[0] // 4
+    shards = [value_weight, gate_weight, out_weight.T, ffn_gate_weight, ffn_up_weight, down_weight.T]
+    cols = vg_cols + out_cols + gu_cols + dn_cols
+    shard_rows = value_weight.shape[0]
+    mine, theirs = whole_call(
+        prep_kernel,
+        [((shard_rows, cols), bf16)] * 2,
+        [
+            jnp.stack([z, 2 * zh + 1 - zl]).astype(jnp.int32),
+            *[pltpu.with_memory_space_constraint(w, pltpu.HBM) for w in shards],
+        ],
+        scratch=[pltpu.SemaphoreType.DMA((12,))],
+        flops=1 << 20,
+        space=pltpu.HBM,
+    )
+    along_x = ring(mine, "x")
+    along_y = ring(swap(theirs, "zl"), "y")
+
+    def second(start, size):
+        cut = lambda pieces: jnp.stack([lax.slice_in_dim(p, start, start + size, axis=1) for p in pieces])
+        return ring(cut(along_x), "y"), ring(cut(along_y), "x")
+
+    split = vg_cols + out_cols
+    vg, outw = ordered([second(0, split)], (vg_cols, out_cols))
+    first, last = second(split, cols - split)
+    others = [[swap(p, "tp") for p in side] for side in (first, last)]
+    ffn_own, ffn_other = ordered([(first, last), others], (cols - split,))
     xs = ring(tok2, Z)
-
-    gu_mine, gu_theirs = mine_theirs(ffn_gate_weight, ffn_up_weight)
-    dn_mine, dn_theirs = mine_theirs(down_weight.T)
-    gu_cols, dn_cols = gu_mine.shape[1], dn_mine.shape[1]
-    pair = paired(jnp.concatenate([gu_mine, dn_mine], axis=1), jnp.concatenate([gu_theirs, dn_theirs], axis=1))
-    gu, down = ordered(*two_ways(pair), (gu_cols, dn_cols))
 
     small = jnp.concatenate([conv_taps, head_gain[None]], axis=0)
     small = lax.dynamic_slice_in_dim(small, z * ch, ch, axis=1)
@@ -272,16 +266,18 @@
         scratch=[pltpu.VMEM((2, rows, 4 * ch), bf16), pltpu.VMEM((rows, width), f32)],
         flops=rows * width * 8 * ch * 2,
     )
-    gu_other, down_other = swap(gu, "tp"), swap(down, "tp")
-    far = [shift_z(normed_ffn, d) for d in SHIFTS]
+    half = rows // 2
+    below = shift_z(normed_ffn, 1)
+    above = shift_z(normed_ffn, 3)
+    opposite = (shift_z(above[:half], 3), shift_z(below[half:], 1))
     ff_flops = rows * width * gu_cols * 6
 
-    def piece(x, kind):
-        (out,) = whole_call(ffn_kernel, [((rows, width), kind)], [x, gu, gu_other, down, down_other], flops=ff_flops)
+    def piece(xs, kind):
+        (out,) = whole_call(ffn_kernel, [((rows, width), kind)], [*xs, ffn_own, ffn_other], flops=ff_flops)
         return out
 
-    returned = [shift_z(piece(x, bf16), -d) for x, d in zip(far, SHIFTS)]
-    fed = piece(normed_ffn, f32)
+    returned = [shift_z(piece(xs, bf16), -d) for xs, d in (((below,), 1), ((above,), 3), (opposite, 2))]
+    fed = piece((normed_ffn,), f32)
     for part in returned:
         fed = fed + part.astype(f32)
     return (middle.astype(f32) + fed).astype(bf16).reshape(tokens.shape)

time: 219 us -> 184 us (0.84)
  Pallas kernels: 41 us -> 18.5 us
  local copies, waits for them, and re-layouts: 6.99 us -> 0.25 us
  waiting for transfers between devices: 88.5 us -> 83 us
  starting transfers between devices: 75.2 us -> 78.4 us
  other arithmetic: 5.2 us -> 2.42 us
    pallas_call x7 -> x10, Pallas kernels: 31.8 us -> 18.5 us  [whole_call(): pl.pallas_call(kernel, out_shape=[jax.ShapeDtypeStruct(s, d) for s, d in...]
    pallas_call x2 -> x0, Pallas kernels: 9.14 us -> none  [ordered(): pl.pallas_call(kernel, out_shape=[jax.ShapeDtypeStruct((2, 4, 4, 64, w),...]
    ppermute x27 -> x21, starting transfers between devices: 38.8 us -> 32.8 us  [ring(): got.append(lax.ppermute(value, axis, [(i, (i + d) % 4) for i in range(4)]))]
    ppermute x9 -> x10, starting transfers between devices: 8.58 us -> 14.1 us  [shift_z(): return lax.ppermute(value, Z, [(i, (i + by) % 4) for i in range(4)])]
    ppermute x27 -> x21, waiting for transfers between devices: 55.4 us -> 50.9 us  [ring(): got.append(lax.ppermute(value, axis, [(i, (i + d) % 4) for i in range(4)]))]
    unnamed x30 -> x6, local copies, waits for them, and re-layouts: 4.45 us -> 0.02 us
    ppermute x8 -> x13, starting transfers between devices: 27.9 us -> 31.5 us  [swap(): return lax.ppermute(value, axis, [(0, 1), (1, 0)])]
    ppermute x8 -> x13, waiting for transfers between devices: 3.01 us -> 0.03 us  [swap(): return lax.ppermute(value, axis, [(0, 1), (1, 0)])]
  transfers between devices with their start and end apart: 44 -> 44, of which waited for: 19 -> 19; matrix products, arithmetic and copies ran while one was open for 2% -> 1% of each run, Pallas kernels for 19% -> 9%
where the time goes in v1:
time: 184 us; the launch traced here: 183 us
  waiting for transfers between devices  83 us (45%)
  starting transfers between devices  78.4 us (43%)
  Pallas kernels  18.5 us (10%)
  other arithmetic  2.42 us (1%)
    ppermute x21, waiting for transfers between devices, ring(): got.append(lax.ppermute(value, axis, [(i, (i + d) % 4) for i in range(4)]))  50.9 us
    ppermute x21, starting transfers between devices, ring(): got.append(lax.ppermute(value, axis, [(i, (i + d) % 4) for i in range(4)]))  32.8 us
    ppermute x10, waiting for transfers between devices, shift_z(): return lax.ppermute(value, Z, [(i, (i + by) % 4) for i in range(4)])  32.1 us
    ppermute x13, starting transfers between devices, swap(): return lax.ppermute(value, axis, [(0, 1), (1, 0)])  31.5 us
    pallas_call x10, Pallas kernels, whole_call(): pl.pallas_call(kernel, out_shape=[jax.ShapeDtypeStruct(s, d) for s, d in...  18.5 us
    ppermute x10, starting transfers between devices, shift_z(): return lax.ppermute(value, Z, [(i, (i + by) % 4) for i in range(4)])  14.1 us
  transfers between devices with their start and end apart: 44, of which 19 were waited for; matrix products, arithmetic and copies ran while one was open for 1% of the time, Pallas kernels for 9%

profile of v1, /device:TPU:1, one launch (start us, length us, event | category | flops | bytes accessed | tf_op | source)
XLA Modules:
  0.0 182.9 jit_solution(929564456989707739)
XLA Ops:
  1.8 3.6 %collective-permute-start.5 = (bf16[64,1920]{1,0:T(8,128)(2,1)S(1)}, bf16[64,1920]{1,0:T(8,128)(2,1)S(1)}, u32[]{:S(2)}, u32[]{:S(2)}) collective-permute-start(bf16[64,1920]{1,0:T(8,128)(2,1)S(1)} %get-tuple-element.13), channel_id=1, source_target_pairs={{0,4},{2,6},{4,0},{6,2},{1,5},{3,7},{5,1},{7,3},{8,12},{10,14},{12... | collective-permute-start | bytes 737288 | tf_op jit(solution)/shard_map/ppermute | solution.py:32
  10.7 5.7 %collective-permute-done.4 = bf16[64,1920]{1,0:T(8,128)(2,1)S(1)} collective-permute-done((bf16[64,1920]{1,0:T(8,128)(2,1)S(1)}, bf16[64,1920]{1,0:T(8,128)(2,1)S(1)}, u32[]{:S(2)}, u32[]{:S(2)}) %collective-permute-start.4) | collective-permute-done | bytes 245792 | tf_op jit(solution)/shard_map/ppermute | solution.py:32
  23.8 18.1 %collective-permute-done.10 = bf16[64,1920]{1,0:T(8,128)(2,1)S(1)} collective-permute-done((bf16[64,1920]{1,0:T(8,128)(2,1)S(1)}, bf16[64,1920]{1,0:T(8,128)(2,1)S(1)}, u32[]{:S(2)}, u32[]{:S(2)}) %collective-permute-start.10) | collective-permute-done | bytes 245792 | tf_op jit(solution)/shard_map/ppermute | solution.py:32
  43.3 5.0 %collective-permute-done.12 = bf16[64,1920]{1,0:T(8,128)(2,1)S(1)} collective-permute-done((bf16[64,1920]{1,0:T(8,128)(2,1)S(1)}, bf16[64,1920]{1,0:T(8,128)(2,1)S(1)}, u32[]{:S(2)}, u32[]{:S(2)}) %collective-permute-start.12) | collective-permute-done | bytes 245792 | tf_op jit(solution)/shard_map/ppermute | solution.py:32
  55.2 2.2 %collective-permute-start.1 = (bf16[128,2048]{1,0:T(8,128)(2,1)S(1)}, bf16[128,2048]{1,0:T(8,128)(2,1)S(1)}, u32[]{:S(2)}, u32[]{:S(2)}) collective-permute-start(bf16[128,2048]{1,0:T(8,128)(2,1)S(1)} %bitcast.55), channel_id=1, source_target_pairs={{0,96},{32,0},{64,32},{96,64},{1,97},{33,1},{65,33},{97,65},{2,98}... | collective-permute-start | bytes 1572872 | tf_op jit(solution)/shard_map/ppermute | solution.py:32
  59.4 3.6 %collective-permute-start.2 = (bf16[128,2048]{1,0:T(8,128)(2,1)S(1)}, bf16[128,2048]{1,0:T(8,128)(2,1)S(1)}, u32[]{:S(2)}, u32[]{:S(2)}) collective-permute-start(bf16[128,2048]{1,0:T(8,128)(2,1)S(1)} %bitcast.56), channel_id=1, source_target_pairs={{0,64},{32,96},{64,0},{96,32},{1,65},{33,97},{65,1},{97,33},{2,66}... | collective-permute-start | bytes 1572872 | tf_op jit(solution)/shard_map/ppermute | solution.py:32
  63.0 5.7 %collective-permute-done.15.refs_7_ = bf16[4,64,768]{2,1,0:T(8,128)(2,1)S(1)} collective-permute-done((bf16[4,64,768]{2,1,0:T(8,128)(2,1)S(1)}, bf16[4,64,768]{2,1,0:T(8,128)(2,1)S(1)}, u32[]{:S(2)}, u32[]{:S(2)}) %collective-permute-start.15) | collective-permute-done | bytes 393248 | tf_op jit(solution)/shard_map/ppermute | solution.py:32
  69.5 2.8 %collective-permute-start.22 = (bf16[2,4,4,64,512]{4,3,2,1,0:T(8,128)(2,1)S(1)}, bf16[2,4,4,64,512]{4,3,2,1,0:T(8,128)(2,1)S(1)}, u32[]{:S(2)}, u32[]{:S(2)}) collective-permute-start(bf16[2,4,4,64,512]{4,3,2,1,0:T(8,128)(2,1)S(1)} %get-tuple-element.16.wa), channel_id=1, source_target_pairs={{0,1},{1,0},{2,3},{3,2},{4,5},{5,4},{6,7},{7,6},{8,9},{9,8},{10,11... | collective-permute-start | bytes 6291464 | tf_op jit(solution)/shard_map/ppermute | solution.py:22
  72.6 2.7 %collective-permute-start.24 = (bf16[4,64,1152]{2,1,0:T(8,128)(2,1)S(1)}, bf16[4,64,1152]{2,1,0:T(8,128)(2,1)S(1)}, u32[]{:S(2)}, u32[]{:S(2)}) collective-permute-start(bf16[4,64,1152]{2,1,0:T(8,128)(2,1)S(1)} %pad_maximum_fusion.refs_0_), channel_id=1, source_target_pairs={{0,24},{8,0},{16,8},{24,16},{1,25},{9,1},{17,9},{25,17},{2,26},{10... | collective-permute-start | bytes 1769480 | tf_op jit(solution)/shard_map/ppermute | solution.py:32
  75.2 3.8 %collective-permute-done.2.x3 = bf16[128,2048]{1,0:T(8,128)(2,1)S(1)} collective-permute-done((bf16[128,2048]{1,0:T(8,128)(2,1)S(1)}, bf16[128,2048]{1,0:T(8,128)(2,1)S(1)}, u32[]{:S(2)}, u32[]{:S(2)}) %collective-permute-start.2) | collective-permute-done | bytes 524320 | tf_op jit(solution)/shard_map/ppermute | solution.py:32
  79.0 3.6 %collective-permute-start.18 = (f32[32,128]{1,0:T(8,128)S(1)}, f32[32,128]{1,0:T(8,128)S(1)}, u32[]{:S(2)}, u32[]{:S(2)}) collective-permute-start(f32[32,128]{1,0:T(8,128)S(1)} %fusion.1), channel_id=1, source_target_pairs={{0,1},{1,0},{2,3},{3,2},{4,5},{5,4},{6,7},{7,6},{8,9},{9,8},{10,11... | collective-permute-start | bytes 49160 | tf_op jit(solution)/shard_map/ppermute | solution.py:22
  85.3 4.0 %collective-permute-done.23.refs_1_ = bf16[4,64,1152]{2,1,0:T(8,128)(2,1)S(1)} collective-permute-done((bf16[4,64,1152]{2,1,0:T(8,128)(2,1)S(1)}, bf16[4,64,1152]{2,1,0:T(8,128)(2,1)S(1)}, u32[]{:S(2)}, u32[]{:S(2)}) %collective-permute-start.23) | collective-permute-done | bytes 589856 | tf_op jit(solution)/shard_map/ppermute | solution.py:32
  89.3 12.8 %collective-permute-start.17 = (bf16[4,16,256]{2,1,0:T(8,128)(2,1)S(1)}, bf16[4,16,256]{2,1,0:T(8,128)(2,1)S(1)}, u32[]{:S(2)}, u32[]{:S(2)}) collective-permute-start(bf16[4,16,256]{2,1,0:T(8,128)(2,1)S(1)} %constant_dynamic-slice_fusion), channel_id=1, source_target_pairs={{0,1},{1,0},{2,3},{3,2},{4,5},{5,4},{6,7},{7,6},{8,9},{9,8},{10,11... | collective-permute-start | bytes 98312 | tf_op jit(solution)/shard_map/ppermute | solution.py:22
  105.0 3.3 %shard_map.112 = bf16[4,128,256]{2,1,0:T(8,128)(2,1)S(1)} custom-call(s32[1]{0:T(128)} %bitcast.1.tp, bf16[4,128,256]{2,1,0:T(8,128)(2,1)S(1)} %shard_map.111.glu, bf16[4,16,256]{2,1,0:T(8,128)(2,1)S(1)} %collective-permute-done.17.edge, f32[32,256]{1,0:T(8,128)S(1)} %pad_maximum_fusion.4.small), custom_call_target="tpu_custom_call" | custom-call | flops 8388608 | bytes 1048576 | tf_op jit(solution)/shard_map/pallas_call | solution.py:70
  108.3 4.0 %collective-permute-start.19 = (bf16[128,256]{1,0:T(8,128)(2,1)S(1)}, bf16[128,256]{1,0:T(8,128)(2,1)S(1)}, u32[]{:S(2)}, u32[]{:S(2)}) collective-permute-start(bf16[128,256]{1,0:T(8,128)(2,1)S(1)} %get-tuple-element.23), channel_id=1, source_target_pairs={{0,96},{32,0},{64,32},{96,64},{1,97},{33,1},{65,33},{97,65},{2,98}... | collective-permute-start | bytes 196616 | tf_op jit(solution)/shard_map/ppermute | solution.py:26
  114.6 2.4 %collective-permute-done.20.a2 = bf16[128,256]{1,0:T(8,128)(2,1)S(1)} collective-permute-done((bf16[128,256]{1,0:T(8,128)(2,1)S(1)}, bf16[128,256]{1,0:T(8,128)(2,1)S(1)}, u32[]{:S(2)}, u32[]{:S(2)}) %collective-permute-start.20) | collective-permute-done | bytes 65568 | tf_op jit(solution)/shard_map/ppermute | solution.py:26
  119.0 2.6 %collective-permute-start.33 = (bf16[4,64,1152]{2,1,0:T(8,128)(2,1)S(1)}, bf16[4,64,1152]{2,1,0:T(8,128)(2,1)S(1)}, u32[]{:S(2)}, u32[]{:S(2)}) collective-permute-start(bf16[4,64,1152]{2,1,0:T(8,128)(2,1)S(1)} %pad_maximum_fusion.1.refs_4_), channel_id=1, source_target_pairs={{0,1},{1,0},{2,3},{3,2},{4,5},{5,4},{6,7},{7,6},{8,9},{9,8},{10,11... | collective-permute-start | bytes 1769480 | tf_op jit(solution)/shard_map/ppermute | solution.py:22
  123.4 2.7 %collective-permute-start.39 = (bf16[128,2048]{1,0:T(8,128)(2,1)S(1)}, bf16[128,2048]{1,0:T(8,128)(2,1)S(1)}, u32[]{:S(2)}, u32[]{:S(2)}) collective-permute-start(bf16[128,2048]{1,0:T(8,128)(2,1)S(1)} %get-tuple-element.18.refs_0_), channel_id=1, source_target_pairs={{0,96},{32,0},{64,32},{96,64},{1,97},{33,1},{65,33},{97,65},{2,98}... | collective-permute-start | bytes 1572872 | tf_op jit(solution)/shard_map/ppermute | solution.py:26
  126.1 5.2 %collective-permute-done.28.refs_7_ = bf16[4,64,1152]{2,1,0:T(8,128)(2,1)S(1)} collective-permute-done((bf16[4,64,1152]{2,1,0:T(8,128)(2,1)S(1)}, bf16[4,64,1152]{2,1,0:T(8,128)(2,1)S(1)}, u32[]{:S(2)}, u32[]{:S(2)}) %collective-permute-start.28) | collective-permute-done | bytes 589856 | tf_op jit(solution)/shard_map/ppermute | solution.py:32
  131.3 3.9 %collective-permute-start.31 = (bf16[4,64,1152]{2,1,0:T(8,128)(2,1)S(1)}, bf16[4,64,1152]{2,1,0:T(8,128)(2,1)S(1)}, u32[]{:S(2)}, u32[]{:S(2)}) collective-permute-start(bf16[4,64,1152]{2,1,0:T(8,128)(2,1)S(1)} %collective-permute-done.24.refs_2_), channel_id=1, source_target_pairs={{0,1},{1,0},{2,3},{3,2},{4,5},{5,4},{6,7},{7,6},{8,9},{9,8},{10,11... | collective-permute-start | bytes 1769480 | tf_op jit(solution)/shard_map/ppermute | solution.py:22
  139.0 7.3 %collective-permute-done.39.refs_0_ = bf16[128,2048]{1,0:T(8,128)(2,1)S(1)} collective-permute-done((bf16[128,2048]{1,0:T(8,128)(2,1)S(1)}, bf16[128,2048]{1,0:T(8,128)(2,1)S(1)}, u32[]{:S(2)}, u32[]{:S(2)}) %collective-permute-start.39) | collective-permute-done | bytes 524320 | tf_op jit(solution)/shard_map/ppermute | solution.py:26
  163.2 4.0 %collective-permute-done.38 = bf16[128,2048]{1,0:T(8,128)(2,1)S(1)} collective-permute-done((bf16[128,2048]{1,0:T(8,128)(2,1)S(1)}, bf16[128,2048]{1,0:T(8,128)(2,1)S(1)}, u32[]{:S(2)}, u32[]{:S(2)}) %collective-permute-start.38) | collective-permute-done | bytes 524320 | tf_op jit(solution)/shard_map/ppermute | solution.py:26
  167.2 3.0 %collective-permute-done.40 = bf16[128,2048]{1,0:T(8,128)(2,1)S(1)} collective-permute-done((bf16[128,2048]{1,0:T(8,128)(2,1)S(1)}, bf16[128,2048]{1,0:T(8,128)(2,1)S(1)}, u32[]{:S(2)}, u32[]{:S(2)}) %collective-permute-start.40) | collective-permute-done | bytes 524320 | tf_op jit(solution)/shard_map/ppermute | solution.py:26
  170.2 11.6 %collective-permute-done.43 = bf16[128,2048]{1,0:T(8,128)(2,1)S(1)} collective-permute-done((bf16[128,2048]{1,0:T(8,128)(2,1)S(1)}, bf16[128,2048]{1,0:T(8,128)(2,1)S(1)}, u32[]{:S(2)}, u32[]{:S(2)}) %collective-permute-start.43) | collective-permute-done | bytes 524320 | tf_op jit(solution)/shard_map/ppermute | solution.py:26
  (109 shorter events, 58.9 us)
Async XLA Ops:
  6.9 14.7 %collective-permute-start.9 = (bf16[64,1920]{1,0:T(8,128)(2,1)S(1)}, bf16[64,1920]{1,0:T(8,128)(2,1)S(1)}, u32[]{:S(2)}, u32[]{:S(2)}) collective-permute-start(bf16[64,1920]{1,0:T(8,128)(2,1)S(1)} %get-tuple-element.14), channel_id=1, source_target_pairs={{0,32},{32,0},{1,33},{33,1},{2,34},{34,2},{3,35},{35,3},{4,36},{36... | collective-permute-start | bytes 737288 | tf_op jit(solution)/shard_map/ppermute | solution.py:22
  16.7 35.2 %collective-permute-start.6 = (bf16[4,64,768]{2,1,0:T(8,128)(2,1)S(1)}, bf16[4,64,768]{2,1,0:T(8,128)(2,1)S(1)}, u32[]{:S(2)}, u32[]{:S(2)}) collective-permute-start(bf16[4,64,768]{2,1,0:T(8,128)(2,1)S(1)} %pad_maximum_fusion.2.refs_0_), channel_id=1, source_target_pairs={{0,8},{8,16},{16,24},{24,0},{1,9},{9,17},{17,25},{25,1},{2,10},{10... | collective-permute-start | bytes 1179656 | tf_op jit(solution)/shard_map/ppermute | solution.py:32
  18.4 35.1 %collective-permute-start.7 = (bf16[4,64,768]{2,1,0:T(8,128)(2,1)S(1)}, bf16[4,64,768]{2,1,0:T(8,128)(2,1)S(1)}, u32[]{:S(2)}, u32[]{:S(2)}) collective-permute-start(bf16[4,64,768]{2,1,0:T(8,128)(2,1)S(1)} %pad_maximum_fusion.2.refs_0_), channel_id=1, source_target_pairs={{0,24},{8,0},{16,8},{24,16},{1,25},{9,1},{17,9},{25,17},{2,26},{10... | collective-permute-start | bytes 1179656 | tf_op jit(solution)/shard_map/ppermute | solution.py:32
  20.0 35.3 %collective-permute-start.8 = (bf16[4,64,768]{2,1,0:T(8,128)(2,1)S(1)}, bf16[4,64,768]{2,1,0:T(8,128)(2,1)S(1)}, u32[]{:S(2)}, u32[]{:S(2)}) collective-permute-start(bf16[4,64,768]{2,1,0:T(8,128)(2,1)S(1)} %pad_maximum_fusion.2.refs_0_), channel_id=1, source_target_pairs={{0,16},{8,24},{16,0},{24,8},{1,17},{9,25},{17,1},{25,9},{2,18},{10... | collective-permute-start | bytes 1179656 | tf_op jit(solution)/shard_map/ppermute | solution.py:32
  21.6 20.3 %collective-permute-start.10 = (bf16[64,1920]{1,0:T(8,128)(2,1)S(1)}, bf16[64,1920]{1,0:T(8,128)(2,1)S(1)}, u32[]{:S(2)}, u32[]{:S(2)}) collective-permute-start(bf16[64,1920]{1,0:T(8,128)(2,1)S(1)} %collective-permute-done.9), channel_id=1, source_target_pairs={{0,8},{8,16},{16,24},{24,0},{1,9},{9,17},{17,25},{25,1},{2,10},{10... | collective-permute-start | bytes 737288 | tf_op jit(solution)/shard_map/ppermute | solution.py:32
  22.1 26.1 %collective-permute-start.12 = (bf16[64,1920]{1,0:T(8,128)(2,1)S(1)}, bf16[64,1920]{1,0:T(8,128)(2,1)S(1)}, u32[]{:S(2)}, u32[]{:S(2)}) collective-permute-start(bf16[64,1920]{1,0:T(8,128)(2,1)S(1)} %collective-permute-done.9), channel_id=1, source_target_pairs={{0,16},{8,24},{16,0},{24,8},{1,17},{9,25},{17,1},{25,9},{2,18},{10... | collective-permute-start | bytes 737288 | tf_op jit(solution)/shard_map/ppermute | solution.py:32
  51.9 16.8 %collective-permute-start.15 = (bf16[4,64,768]{2,1,0:T(8,128)(2,1)S(1)}, bf16[4,64,768]{2,1,0:T(8,128)(2,1)S(1)}, u32[]{:S(2)}, u32[]{:S(2)}) collective-permute-start(bf16[4,64,768]{2,1,0:T(8,128)(2,1)S(1)} %pad_maximum_fusion.3.refs_4_), channel_id=1, source_target_pairs={{0,4},{2,6},{4,0},{6,2},{1,5},{3,7},{5,1},{7,3},{8,12},{10,14},{12... | collective-permute-start | bytes 1179656 | tf_op jit(solution)/shard_map/ppermute | solution.py:32
  53.5 18.9 %collective-permute-start = (bf16[128,2048]{1,0:T(8,128)(2,1)S(1)}, bf16[128,2048]{1,0:T(8,128)(2,1)S(1)}, u32[]{:S(2)}, u32[]{:S(2)}) collective-permute-start(bf16[128,2048]{1,0:T(8,128)(2,1)S(1)} %bitcast.54), channel_id=1, source_target_pairs={{0,32},{32,64},{64,96},{96,0},{1,33},{33,65},{65,97},{97,1},{2,34}... | collective-permute-start | bytes 1572872 | tf_op jit(solution)/shard_map/ppermute | solution.py:32
  55.2 17.3 %collective-permute-start.1 = (bf16[128,2048]{1,0:T(8,128)(2,1)S(1)}, bf16[128,2048]{1,0:T(8,128)(2,1)S(1)}, u32[]{:S(2)}, u32[]{:S(2)}) collective-permute-start(bf16[128,2048]{1,0:T(8,128)(2,1)S(1)} %bitcast.55), channel_id=1, source_target_pairs={{0,96},{32,0},{64,32},{96,64},{1,97},{33,1},{65,33},{97,65},{2,98}... | collective-permute-start | bytes 1572872 | tf_op jit(solution)/shard_map/ppermute | solution.py:32
  59.4 19.7 %collective-permute-start.2 = (bf16[128,2048]{1,0:T(8,128)(2,1)S(1)}, bf16[128,2048]{1,0:T(8,128)(2,1)S(1)}, u32[]{:S(2)}, u32[]{:S(2)}) collective-permute-start(bf16[128,2048]{1,0:T(8,128)(2,1)S(1)} %bitcast.56), channel_id=1, source_target_pairs={{0,64},{32,96},{64,0},{96,32},{1,65},{33,97},{65,1},{97,33},{2,66}... | collective-permute-start | bytes 1572872 | tf_op jit(solution)/shard_map/ppermute | solution.py:32
  69.5 52.1 %collective-permute-start.22 = (bf16[2,4,4,64,512]{4,3,2,1,0:T(8,128)(2,1)S(1)}, bf16[2,4,4,64,512]{4,3,2,1,0:T(8,128)(2,1)S(1)}, u32[]{:S(2)}, u32[]{:S(2)}) collective-permute-start(bf16[2,4,4,64,512]{4,3,2,1,0:T(8,128)(2,1)S(1)} %get-tuple-element.16.wa), channel_id=1, source_target_pairs={{0,1},{1,0},{2,3},{3,2},{4,5},{5,4},{6,7},{7,6},{8,9},{9,8},{10,11... | collective-permute-start | bytes 6291464 | tf_op jit(solution)/shard_map/ppermute | solution.py:22
  72.5 16.8 %collective-permute-start.23 = (bf16[4,64,1152]{2,1,0:T(8,128)(2,1)S(1)}, bf16[4,64,1152]{2,1,0:T(8,128)(2,1)S(1)}, u32[]{:S(2)}, u32[]{:S(2)}) collective-permute-start(bf16[4,64,1152]{2,1,0:T(8,128)(2,1)S(1)} %pad_maximum_fusion.refs_0_), channel_id=1, source_target_pairs={{0,8},{8,16},{16,24},{24,0},{1,9},{9,17},{17,25},{25,1},{2,10},{10... | collective-permute-start | bytes 1769480 | tf_op jit(solution)/shard_map/ppermute | solution.py:32
  72.6 29.7 %collective-permute-start.24 = (bf16[4,64,1152]{2,1,0:T(8,128)(2,1)S(1)}, bf16[4,64,1152]{2,1,0:T(8,128)(2,1)S(1)}, u32[]{:S(2)}, u32[]{:S(2)}) collective-permute-start(bf16[4,64,1152]{2,1,0:T(8,128)(2,1)S(1)} %pad_maximum_fusion.refs_0_), channel_id=1, source_target_pairs={{0,24},{8,0},{16,8},{24,16},{1,25},{9,1},{17,9},{25,17},{2,26},{10... | collective-permute-start | bytes 1769480 | tf_op jit(solution)/shard_map/ppermute | solution.py:32
  82.7 25.7 %collective-permute-start.25 = (bf16[4,64,1152]{2,1,0:T(8,128)(2,1)S(1)}, bf16[4,64,1152]{2,1,0:T(8,128)(2,1)S(1)}, u32[]{:S(2)}, u32[]{:S(2)}) collective-permute-start(bf16[4,64,1152]{2,1,0:T(8,128)(2,1)S(1)} %pad_maximum_fusion.refs_0_), channel_id=1, source_target_pairs={{0,16},{8,24},{16,0},{24,8},{1,17},{9,25},{17,1},{25,9},{2,18},{10... | collective-permute-start | bytes 1769480 | tf_op jit(solution)/shard_map/ppermute | solution.py:32
  84.9 27.4 %collective-permute-start.29 = (bf16[4,64,1152]{2,1,0:T(8,128)(2,1)S(1)}, bf16[4,64,1152]{2,1,0:T(8,128)(2,1)S(1)}, u32[]{:S(2)}, u32[]{:S(2)}) collective-permute-start(bf16[4,64,1152]{2,1,0:T(8,128)(2,1)S(1)} %pad_maximum_fusion.refs_0_), channel_id=1, source_target_pairs={{0,1},{1,0},{2,3},{3,2},{4,5},{5,4},{6,7},{7,6},{8,9},{9,8},{10,11... | collective-permute-start | bytes 1769480 | tf_op jit(solution)/shard_map/ppermute | solution.py:22
  102.2 21.1 %collective-permute-start.26 = (bf16[4,64,1152]{2,1,0:T(8,128)(2,1)S(1)}, bf16[4,64,1152]{2,1,0:T(8,128)(2,1)S(1)}, u32[]{:S(2)}, u32[]{:S(2)}) collective-permute-start(bf16[4,64,1152]{2,1,0:T(8,128)(2,1)S(1)} %pad_maximum_fusion.1.refs_4_), channel_id=1, source_target_pairs={{0,2},{2,4},{4,6},{6,0},{1,3},{3,5},{5,7},{7,1},{8,10},{10,12},{12... | collective-permute-start | bytes 1769480 | tf_op jit(solution)/shard_map/ppermute | solution.py:32
  103.2 20.3 %collective-permute-start.27 = (bf16[4,64,1152]{2,1,0:T(8,128)(2,1)S(1)}, bf16[4,64,1152]{2,1,0:T(8,128)(2,1)S(1)}, u32[]{:S(2)}, u32[]{:S(2)}) collective-permute-start(bf16[4,64,1152]{2,1,0:T(8,128)(2,1)S(1)} %pad_maximum_fusion.1.refs_4_), channel_id=1, source_target_pairs={{0,6},{2,0},{4,2},{6,4},{1,7},{3,1},{5,3},{7,5},{8,14},{10,8},{12,... | collective-permute-start | bytes 1769480 | tf_op jit(solution)/shard_map/ppermute | solution.py:32
  117.0 14.4 %collective-permute-start.28 = (bf16[4,64,1152]{2,1,0:T(8,128)(2,1)S(1)}, bf16[4,64,1152]{2,1,0:T(8,128)(2,1)S(1)}, u32[]{:S(2)}, u32[]{:S(2)}) collective-permute-start(bf16[4,64,1152]{2,1,0:T(8,128)(2,1)S(1)} %pad_maximum_fusion.1.refs_4_), channel_id=1, source_target_pairs={{0,4},{2,6},{4,0},{6,2},{1,5},{3,7},{5,1},{7,3},{8,12},{10,14},{12... | collective-permute-start | bytes 1769480 | tf_op jit(solution)/shard_map/ppermute | solution.py:32
  119.0 16.3 %collective-permute-start.33 = (bf16[4,64,1152]{2,1,0:T(8,128)(2,1)S(1)}, bf16[4,64,1152]{2,1,0:T(8,128)(2,1)S(1)}, u32[]{:S(2)}, u32[]{:S(2)}) collective-permute-start(bf16[4,64,1152]{2,1,0:T(8,128)(2,1)S(1)} %pad_maximum_fusion.1.refs_4_), channel_id=1, source_target_pairs={{0,1},{1,0},{2,3},{3,2},{4,5},{5,4},{6,7},{7,6},{8,9},{9,8},{10,11... | collective-permute-start | bytes 1769480 | tf_op jit(solution)/shard_map/ppermute | solution.py:22
  123.4 22.8 %collective-permute-start.39 = (bf16[128,2048]{1,0:T(8,128)(2,1)S(1)}, bf16[128,2048]{1,0:T(8,128)(2,1)S(1)}, u32[]{:S(2)}, u32[]{:S(2)}) collective-permute-start(bf16[128,2048]{1,0:T(8,128)(2,1)S(1)} %get-tuple-element.18.refs_0_), channel_id=1, source_target_pairs={{0,96},{32,0},{64,32},{96,64},{1,97},{33,1},{65,33},{97,65},{2,98}... | collective-permute-start | bytes 1572872 | tf_op jit(solution)/shard_map/ppermute | solution.py:26
  131.3 16.7 %collective-permute-start.31 = (bf16[4,64,1152]{2,1,0:T(8,128)(2,1)S(1)}, bf16[4,64,1152]{2,1,0:T(8,128)(2,1)S(1)}, u32[]{:S(2)}, u32[]{:S(2)}) collective-permute-start(bf16[4,64,1152]{2,1,0:T(8,128)(2,1)S(1)} %collective-permute-done.24.refs_2_), channel_id=1, source_target_pairs={{0,1},{1,0},{2,3},{3,2},{4,5},{5,4},{6,7},{7,6},{8,9},{9,8},{10,11... | collective-permute-start | bytes 1769480 | tf_op jit(solution)/shard_map/ppermute | solution.py:22
  135.3 14.3 %collective-permute-start.34 = (bf16[4,64,1152]{2,1,0:T(8,128)(2,1)S(1)}, bf16[4,64,1152]{2,1,0:T(8,128)(2,1)S(1)}, u32[]{:S(2)}, u32[]{:S(2)}) collective-permute-start(bf16[4,64,1152]{2,1,0:T(8,128)(2,1)S(1)} %collective-permute-done.26.refs_5_), channel_id=1, source_target_pairs={{0,1},{1,0},{2,3},{3,2},{4,5},{5,4},{6,7},{7,6},{8,9},{9,8},{10,11... | collective-permute-start | bytes 1769480 | tf_op jit(solution)/shard_map/ppermute | solution.py:22
  152.9 14.3 %collective-permute-start.38 = (bf16[128,2048]{1,0:T(8,128)(2,1)S(1)}, bf16[128,2048]{1,0:T(8,128)(2,1)S(1)}, u32[]{:S(2)}, u32[]{:S(2)}) collective-permute-start(bf16[128,2048]{1,0:T(8,128)(2,1)S(1)} %shard_map.116), channel_id=1, source_target_pairs={{0,96},{32,0},{64,32},{96,64},{1,97},{33,1},{65,33},{97,65},{2,98}... | collective-permute-start | bytes 1572872 | tf_op jit(solution)/shard_map/ppermute | solution.py:26
  159.0 22.7 %collective-permute-start.43 = (bf16[128,2048]{1,0:T(8,128)(2,1)S(1)}, bf16[128,2048]{1,0:T(8,128)(2,1)S(1)}, u32[]{:S(2)}, u32[]{:S(2)}) collective-permute-start(bf16[128,2048]{1,0:T(8,128)(2,1)S(1)} %shard_map.118), channel_id=1, source_target_pairs={{0,64},{32,96},{64,0},{96,32},{1,65},{33,97},{65,1},{97,33},{2,66}... | collective-permute-start | bytes 1572872 | tf_op jit(solution)/shard_map/ppermute | solution.py:26
  (23 other events, 365.1 us)
